TPU v7x, 256 devices: a 4x2x16 block of a 4x16x16 slice. The times are simulated.
256 devices in a mesh: grp: 2 (over y), ep: 32 (over z, core), tp: 4 (over x).
Axes of the slice: x: 4, y: 2, z: 16, core: 2. Of those that a mesh axis runs over, the one named last changes fastest.
The devices are a block of a 4x16x16 slice.
Arguments:
- query_first: bfloat16 [24576, 512], P(('grp', 'ep'), 'tp'), parts along dimension 0, may hold values from -32 to 32
- query_second: bfloat16 [24576, 512], P(('grp', 'ep'), 'tp'), parts along dimension 0, may hold values from -32 to 32
- key_first: bfloat16 [24576, 512], P(('grp', 'ep'), 'tp'), parts along dimension 0, may hold values from -32 to 32
- key_second: bfloat16 [24576, 512], P(('grp', 'ep'), 'tp'), parts along dimension 0, may hold values from -32 to 32
- values: bfloat16 [24576, 1024], P(('grp', 'ep'), 'tp'), parts along dimension 0, may hold values from -6 to 6
- lambda_head: float32 [8], P('tp'), may hold values from 0.3 to 0.8
- head_gain: float32 [128], replicated, may hold values from 0.1 to 1.9
- out_weight: bfloat16 [1024, 2048], replicated, may hold values from -0.1875 to 0.1875
- tokens: bfloat16 [32768, 2048], P(('grp', 'ep', 'tp')), parts along dimension 0, may hold values from -6 to 6
- norm_gain: float32 [2048], replicated, may hold values from 0.1 to 1.9
- expert_ids: int32 [32768, 2], P(('grp', 'ep', 'tp')), parts along dimension 0, may hold values from 0 to 31, all different within a row; in each aligned block of 128 rows (0 to 127, 128 to 255, ...) at most 12 rows name the same one
- expert_weights: float32 [32768, 2], P(('grp', 'ep', 'tp')), parts along dimension 0, may hold values from 0.2 to 1
- expert_gate: bfloat16 [32, 2048, 1024], P('ep', None, 'tp'), may hold values from -0.125 to 0.125
- expert_up: bfloat16 [32, 2048, 1024], P('ep', None, 'tp'), may hold values from -0.125 to 0.125
- expert_down: bfloat16 [32, 1024, 2048], P('ep', 'tp'), may hold values from -0.1875 to 0.1875
- shared_gate: bfloat16 [2048, 512], P(None, 'tp'), may hold values from -0.125 to 0.125
- shared_up: bfloat16 [2048, 512], P(None, 'tp'), may hold values from -0.125 to 0.125
- shared_down: bfloat16 [512, 2048], P('tp'), may hold values from -0.25 to 0.25
Outputs:
- mixed: bfloat16 [24576, 2048], P(('grp', 'ep', 'tp')), parts along dimension 0
- expert_out: bfloat16 [32768, 2048], P(('grp', 'ep', 'tp')), parts along dimension 0
There are 2 independent parts, one for each index of `grp`. A program takes and returns all parts, laid end to end along the dimension named above; an argument that names none is the same for every part. Nothing has to cross between parts.
Inputs may be any that keep to these rules, and one draw needn't show every extreme that they name: `expert_ids`: in the rows of one device (aligned blocks of 128 rows) no expert is named by more than 12 rows, and in every draw some expert is named by exactly 12 rows of some block; each row names 2 different experts.
All inputs are finite; a program needn't handle non-finite values.
Results may differ from a plain program's by a relative error of at most 0.012.
Values may be sent and summed in bfloat16 or wider, within the bound.
A program may use at most 128 MiB of HBM per device.

v0:
```python
import jax
import jax.numpy as jnp
from jax import lax
from jax.sharding import Mesh
from jax.sharding import PartitionSpec as P

EP = ("ep_0", "ep_1")
GRP_EP = ("grp", "ep_0", "ep_1")
GRP_EP_TP = ("grp", "ep_0", "ep_1", "tp")
epsilon = 1e-06
block_limit = 1536


def sent_together(arrays, axis, dim, along):
    widths = [a.shape[along] for a in arrays]
    both = jnp.concatenate(arrays, axis=along)
    filled = lax.all_gather(both, axis, axis=dim, tiled=True)
    return tuple(jnp.split(filled, [sum(widths[:k]) for k in range(1, len(widths))], axis=along))


def in_blocks(value, dim, peers):
    before, after = (value.shape[:dim], value.shape[dim + 1 :])
    return jnp.moveaxis(value.reshape(*before, peers, -1, *after), dim, 0)


def in_order(tiles, dim):
    dims = list(tiles.shape[1:])
    dims[dim] *= tiles.shape[0]
    return jnp.moveaxis(tiles, 0, dim).reshape(dims)


def exchange_in_order(tiles, axes, order):
    dims = [lax.axis_size(a) for a in axes]
    tiles = tiles.reshape(*dims, *tiles.shape[1:])
    for k in order:
        tiles = lax.all_to_all(tiles, axes[k], split_axis=k, concat_axis=k, tiled=True)
    return tiles.reshape(-1, *tiles.shape[len(axes) :])


def two_step_exchange(value, groups, order, split_dim, concat_dim):
    peers = lax.axis_size(groups[0]) * lax.axis_size(groups[1])
    tiles = in_blocks(value, split_dim, peers)
    return in_order(exchange_in_order(tiles, groups, order), concat_dim)


def key_block(total_rows, shard_rows):
    best_rows = shard_rows
    for factor_rows in range(1, total_rows // shard_rows + 1):
        if total_rows % (factor_rows * shard_rows) == 0 and factor_rows * shard_rows <= block_limit:
            best_rows = factor_rows * shard_rows
    return best_rows


def softmax_update(states, scores, value_block):
    running_max, running_sum, accumulated = states
    new_max = jnp.maximum(running_max, jnp.max(scores, axis=-1))
    rescale = jnp.exp(running_max - new_max)
    weights = jnp.exp(scores - new_max[..., None])
    new_sum = running_sum * rescale + jnp.sum(weights, axis=-1)
    product = jnp.einsum(
        "qhk,khe->qhe",
        weights.astype(jnp.bfloat16),
        value_block,
        preferred_element_type=jnp.float32,
    )
    return (new_max, new_sum, accumulated * rescale[..., None] + product)


def shards(
    query_first,
    query_second,
    key_first,
    key_second,
    values,
    lambda_head,
    head_gain,
    out_weight,
    tokens,
    norm_gain,
    expert_ids,
    expert_weights,
    expert_gate,
    expert_up,
    expert_down,
    shared_gate,
    shared_up,
    shared_down,
):
    shard_rows, query_width = query_first.shape
    heads_here = lambda_head.shape[0]
    head_size = query_width // heads_here
    value_size = values.shape[1] // heads_here
    score_scale = head_size ** (-0.5)
    query_one = query_first.reshape(shard_rows, heads_here, head_size)
    query_two = query_second.reshape(shard_rows, heads_here, head_size)
    initial = (
        jnp.full((shard_rows, heads_here), -jnp.inf, jnp.float32),
        jnp.zeros((shard_rows, heads_here), jnp.float32),
        jnp.zeros((shard_rows, heads_here, value_size), jnp.float32),
    )
    carried = (initial, initial)
    key_one, key_two, value_piece = sent_together((key_first, key_second, values), EP, 0, 1)
    total_rows = key_one.shape[0]
    block_rows = key_block(total_rows, shard_rows)
    block_count = total_rows // block_rows
    stacked = (
        key_one.reshape(block_count, block_rows, heads_here, head_size),
        key_two.reshape(block_count, block_rows, heads_here, head_size),
        value_piece.reshape(block_count, block_rows, heads_here, value_size),
    )

    def fold_step(states, blocks):
        first_state, second_state = states
        key_a, key_b, value_block = blocks
        scores_a = (
            jnp.einsum("qhd,khd->qhk", query_one, key_a, preferred_element_type=jnp.float32)
            * score_scale
        )
        scores_b = (
            jnp.einsum("qhd,khd->qhk", query_two, key_b, preferred_element_type=jnp.float32)
            * score_scale
        )
        return (
            (
                softmax_update(first_state, scores_a, value_block),
                softmax_update(second_state, scores_b, value_block),
            ),
            None,
        )

    carried, unused = lax.scan(fold_step, carried, stacked)
    first_state, second_state = carried
    first_out = first_state[2] / first_state[1][..., None]
    second_out = second_state[2] / second_state[1][..., None]
    mixture = first_out - lambda_head[None, :, None] * second_out
    normed_heads = (
        mixture
        * lax.rsqrt(jnp.mean(mixture * mixture, axis=-1, keepdims=True) + epsilon)
        * head_gain
    )
    head_local = normed_heads.astype(jnp.bfloat16).reshape(shard_rows, heads_here * value_size)
    position_heads = lax.all_to_all(head_local, "tp", split_axis=0, concat_axis=1, tiled=True)
    mixed = jnp.dot(position_heads, out_weight, preferred_element_type=jnp.float32).astype(
        jnp.bfloat16
    )
    row_count, model_width = tokens.shape
    top_count = expert_ids.shape[1]
    ep_count = lax.axis_size(EP)
    local_experts = expert_gate.shape[0]
    expert_count = local_experts * ep_count
    capacity = max(2, row_count * top_count * 3 // (2 * expert_count))
    routed_rows = expert_count * capacity
    owner_span = routed_rows + row_count
    widened = tokens.astype(jnp.float32)
    normed = (
        widened
        * lax.rsqrt(jnp.mean(widened * widened, axis=-1, keepdims=True) + epsilon)
        * norm_gain
    ).astype(jnp.bfloat16)
    flat_ids = expert_ids.reshape(-1)
    onehot = (flat_ids[:, None] == jnp.arange(expert_count, dtype=jnp.int32)[None, :]).astype(
        jnp.int32
    )
    ranks = jnp.sum(onehot * jnp.cumsum(onehot, axis=0), axis=1) - 1
    slot_index = flat_ids * capacity + ranks
    token_index = jnp.arange(flat_ids.shape[0], dtype=jnp.int32) // top_count
    filled = jnp.full((routed_rows,), row_count, jnp.int32).at[slot_index].set(token_index)
    padded = jnp.concatenate([normed, jnp.zeros((1, model_width), jnp.bfloat16)], axis=0)
    outgoing = padded[filled].reshape(1, ep_count, local_experts * capacity, model_width)
    arrived = two_step_exchange(outgoing, ("ep_0", "ep_1"), (1, 0), 1, 1)
    local_rows = jnp.concatenate(
        [arrived.reshape(1, routed_rows, model_width), normed[None]], axis=1
    )
    gathered = lax.all_gather(local_rows, "tp", axis=0, tiled=True)
    owners = owner_span * lax.axis_size("tp") // owner_span
    routed_in = gathered[:, :routed_rows].reshape(
        owners, ep_count, local_experts, capacity, model_width
    )
    gate_value = jnp.einsum(
        "osecd,edf->osecf", routed_in, expert_gate, preferred_element_type=jnp.float32
    )
    up_value = jnp.einsum(
        "osecd,edf->osecf", routed_in, expert_up, preferred_element_type=jnp.float32
    )
    hidden = (jax.nn.silu(gate_value) * up_value).astype(jnp.bfloat16)
    routed_out = jnp.einsum(
        "osecf,efd->osecd", hidden, expert_down, preferred_element_type=jnp.float32
    )
    routed_out = routed_out.reshape(owners, routed_rows, model_width)
    shared_in = gathered[:, routed_rows:]
    shared_gate_value = jnp.einsum(
        "ord,df->orf", shared_in, shared_gate, preferred_element_type=jnp.float32
    )
    shared_up_value = jnp.einsum(
        "ord,df->orf", shared_in, shared_up, preferred_element_type=jnp.float32
    )
    shared_hidden = (jax.nn.silu(shared_gate_value) * shared_up_value).astype(jnp.bfloat16)
    shared_out = jnp.einsum(
        "orf,fd->ord", shared_hidden, shared_down, preferred_element_type=jnp.float32
    )
    kept_rows = lax.psum_scatter(
        jnp.concatenate([routed_out, shared_out], axis=1)
        .reshape(owners * owner_span, model_width)
        .astype(jnp.bfloat16),
        "tp",
        scatter_dimension=0,
        tiled=True,
    ).astype(jnp.float32)
    routed_back = (
        kept_rows[:routed_rows]
        .astype(jnp.bfloat16)
        .reshape(ep_count, local_experts * capacity, model_width)
    )
    returned = two_step_exchange(routed_back, ("ep_0", "ep_1"), (1, 0), 0, 0).reshape(
        routed_rows, model_width
    )
    picked = returned[slot_index].reshape(row_count, top_count, model_width).astype(jnp.float32)
    combined = jnp.sum(picked * expert_weights[:, :, None], axis=1) + kept_rows[routed_rows:]
    expert_out = combined.astype(jnp.bfloat16)
    return (mixed, expert_out)


def solution(mesh):
    torus = Mesh(
        mesh.devices.reshape(mesh.shape["grp"], 16, 2, mesh.shape["tp"]),
        ("grp", "ep_0", "ep_1", "tp"),
    )
    placed = (
        P(GRP_EP, "tp"),
        P(GRP_EP, "tp"),
        P(GRP_EP, "tp"),
        P(GRP_EP, "tp"),
        P(GRP_EP, "tp"),
        P("tp"),
        P(),
        P(),
        P(GRP_EP_TP, None),
        P(),
        P(GRP_EP_TP, None),
        P(GRP_EP_TP, None),
        P(EP, None, "tp"),
        P(EP, None, "tp"),
        P(EP, "tp", None),
        P(None, "tp"),
        P(None, "tp"),
        P("tp", None),
    )
    return jax.shard_map(
        shards,
        mesh=torus,
        in_specs=placed,
        out_specs=(P(GRP_EP_TP, None), P(GRP_EP_TP, None)),
        check_vma=False,
    )
```

profile of v0, /device:TPU:40, one launch (start us, length us, event | category | flops | bytes accessed | tf_op | source)
XLA Modules:
  0.0 628.7 jit_solution(13086468374661407831)
XLA Ops:
  14.2 3.1 gather_fusion
  17.3 2.4 reshape_transpose_reshape_reshape.3
  20.6 5.1 all_to_all.39
  25.7 2.8 copy.87
  28.5 24.0 %all-to-all-start.2 = ((bf16[16,2,1,1,12,2048]{5,1,4,3,2,0:T(2,128)(2,1)}), bf16[16,2,1,1,12,2048]{5,1,4,3,2,0:T(2,128)(2,1)}, u32[]{:S(2)}, u32[]{:S(2)}) async-start(bf16[16,2,1,1,12,2048]{5,1,4,3,2,0:T(2,128)(2,1)} %copy.87), calls=%async_computation.2 | async-start | bytes 3145728 | tf_op jit(solution)/shard_map/all_to_all | solution.py:36
  53.6 73.3 %all-to-all-done.2 = bf16[16,2,1,1,12,2048]{5,1,4,3,2,0:T(2,128)(2,1)} async-done(((bf16[16,2,1,1,12,2048]{5,1,4,3,2,0:T(2,128)(2,1)}), bf16[16,2,1,1,12,2048]{5,1,4,3,2,0:T(2,128)(2,1)}, u32[]{:S(2)}, u32[]{:S(2)}) %all-to-all-start.2) | async-done | bytes 1572896 | tf_op jit(solution)/shard_map/all_to_all | solution.py:36
  126.9 2.2 copy.88
  130.4 3.2 pad_maximum_fusion.1
  135.2 83.4 %all-gather.5.cloned.1.call-done = bf16[4,512,2048]{2,1,0:T(8,128)(2,1)} async-done(((bf16[1,512,2048]{2,1,0:T(8,128)(2,1)}), bf16[4,512,2048]{2,1,0:T(8,128)(2,1)}) %all-gather.5.cloned.1.call-update) | async-done | bytes 8388624 | tf_op jit(solution)/shard_map/all_gather | solution.py:174
  218.6 6.5 %slice.34 = bf16[4,384,2048]{2,1,0:T(8,128)(2,1)} slice(bf16[4,512,2048]{2,1,0:T(8,128)(2,1)} %all-gather.5.cloned.1.call-done), slice={[0:4], [0:384], [0:2048]} | slice | bytes 12582912 | tf_op jit(solution)/shard_map/slice | solution.py:176
  225.1 10.4 %copy.89 = bf16[4,384,2048]{2,0,1:T(4,128)(2,1)} copy(bf16[4,384,2048]{2,1,0:T(8,128)(2,1)} %slice.34) | data formatting | bytes 12582912 | tf_op jit(solution)/shard_map/slice | solution.py:176
  235.5 11.6 %fusion.44 = f32[4,32,12,256]{3,1,2,0:T(8,128)} fusion(bf16[4,32,12,2048]{3,0,2,1:T(4,128)(2,1)} %bitcast.191, bf16[1,2048,256]{2,1,0:T(8,128)(2,1)S(1)} %copy-done.15), kind=kOutput, calls=%fused_computation.52 | convolution fusion | flops 1610612736 | bytes 8912896 | tf_op jit(solution)/shard_map/osecd,edf->osecf/dot_general | solution.py:179
  247.2 17.0 %convert_bitcast_fusion = bf16[4,32,1,12,2048]{4,1,3,0,2:T(8,128)(2,1)} fusion(bf16[1,256,2048]{2,1,0:T(8,128)(2,1)S(1)} %copy-done, bf16[4,32,12,2048]{3,0,2,1:T(4,128)(2,1)} %bitcast.192, f32[4,32,12,256]{3,1,2,0:T(8,128)} %fusion.44, bf16[1,2048,256]{2,1,0:T(8,128)(2,1)} %param.33), kind=kOutput, calls=%fused_computation.49 | convolution fusion | flops 3226730496 | bytes 16252928 | tf_op jit(solution)/shard_map/osecf,efd->osecd/dot_general | solution.py:186
  264.2 10.5 %copy.92 = bf16[4,32,1,12,2048]{4,0,3,1,2:T(4,128)(2,1)} copy(bf16[4,32,1,12,2048]{4,1,3,0,2:T(8,128)(2,1)} %convert_bitcast_fusion) | data formatting | bytes 12582912 | tf_op jit(solution)/shard_map/osecf,efd->osecd/transpose | solution.py:186
  274.8 2.4 fusion.48
  277.1 5.3 convolution_convert_fusion
  282.4 3.2 copy.93
  285.7 8.4 %pad_maximum_fusion = bf16[4,512,2048]{2,0,1:T(4,128)(2,1)} fusion(bf16[4,128,2048]{2,0,1:T(4,128)(2,1)S(1)} %copy.93, bf16[4,384,2048]{2,0,1:T(4,128)(2,1)} %bitcast.190), kind=kLoop, calls=%fused_computation.48 | loop fusion | flops 4194304 | bytes 16777216 | tf_op jit(solution)/shard_map/concatenate | solution.py:202
  294.1 11.4 %copy.94 = bf16[4,512,2048]{2,1,0:T(8,128)(2,1)} copy(bf16[4,512,2048]{2,0,1:T(4,128)(2,1)} %pad_maximum_fusion) | data formatting | bytes 16777216 | tf_op jit(solution)/shard_map/concatenate | solution.py:202
  307.3 4.8 fusion.94
  312.1 11.6 %reshape.177 = bf16[8,1536,2,64]{3,2,1,0:T(2,128)(2,1)} reshape(bf16[12288,128]{1,0:T(8,128)(2,1)} %get-tuple-element.183) | data formatting | bytes 6291456 | tf_op jit(solution)/shard_map/reshape | solution.py:107
  323.8 15.5 %copy.77 = bf16[8,1536,2,64]{1,3,2,0:T(8,128)(2,1)} copy(bf16[8,1536,2,64]{3,2,1,0:T(2,128)(2,1)} %reshape.177) | data formatting | bytes 6291456
  339.2 11.6 %reshape.179 = bf16[8,1536,2,64]{3,2,1,0:T(2,128)(2,1)} reshape(bf16[12288,128]{1,0:T(8,128)(2,1)} %get-tuple-element.182) | data formatting | bytes 6291456 | tf_op jit(solution)/shard_map/reshape | solution.py:108
  350.9 15.6 %copy.79 = bf16[8,1536,2,64]{1,3,2,0:T(8,128)(2,1)} copy(bf16[8,1536,2,64]{3,2,1,0:T(2,128)(2,1)} %reshape.179) | data formatting | bytes 6291456
  366.4 6.4 %split.13 = bf16[12288,256]{1,0:T(8,128)(2,1)} slice(bf16[12288,512]{1,0:T(8,128)(2,1)} %all-gather.3.cloned.1.call-done), slice={[0:12288], [256:512]} | slice | bytes 12582912 | tf_op jit(solution)/shard_map/split | solution.py:18
  372.8 9.8 %reshape.178 = bf16[8,1536,2,128]{3,2,1,0:T(2,128)(2,1)} reshape(bf16[12288,256]{1,0:T(8,128)(2,1)} %split.13) | data formatting | bytes 12582912 | tf_op jit(solution)/shard_map/reshape | solution.py:109
  382.6 118.0 %while.21 = (s32[]{:T(128)}, f32[384,2]{0,1:T(2,128)S(1)}, f32[384,2]{0,1:T(2,128)S(1)}, f32[384,2,128]{0,2,1:T(8,128)S(1)}, f32[384,2]{0,1:T(2,128)S(1)}, /*ind...) while((s32[]{:T(128)}, f32[384,2]{0,1:T(2,128)S(1)}, ...), condition=%wide.region_5.6_spmd.clone, body=%wide.region_0.5_spmd.clone.sunk | while | flops 925441536 | bytes 92308720 | solution.py:131
  392.8 3.5 fusion.125
  407.6 3.5 fusion.125
  422.3 3.5 fusion.125
  437.0 3.5 fusion.125
  451.8 3.5 fusion.125
  466.5 3.5 fusion.125
  481.2 3.5 fusion.125
  495.9 3.5 fusion.125
  502.0 2.7 slice.36
  504.7 2.4 reshape_reshape_reshape.6
  508.0 5.0 all_to_all.40
  513.0 4.2 all-to-all-start
  517.2 2.8 copy.96
  520.0 3.6 all-to-all-done
  523.6 10.7 %all-to-all-start.4 = ((bf16[16,2,1,12,2048]{4,1,3,2,0:T(2,128)(2,1)}), bf16[16,2,1,12,2048]{4,1,3,2,0:T(2,128)(2,1)S(1)}, u32[]{:S(2)}, u32[]{:S(2)}) async-start(bf16[16,2,1,12,2048]{4,1,3,2,0:T(2,128)(2,1)} %copy.96), calls=%async_computation.5 | async-start | bytes 3145728 | tf_op jit(solution)/shard_map/all_to_all | solution.py:36
  534.4 3.7 convolution_convert_fusion.1
  538.2 69.0 %all-to-all-done.4 = bf16[16,2,1,12,2048]{4,1,3,2,0:T(2,128)(2,1)S(1)} async-done(((bf16[16,2,1,12,2048]{4,1,3,2,0:T(2,128)(2,1)}), bf16[16,2,1,12,2048]{4,1,3,2,0:T(2,128)(2,1)S(1)}, u32[]{:S(2)}, u32[]{:S(2)}) %all-to-all-start.4) | async-done | bytes 1572896 | tf_op jit(solution)/shard_map/all_to_all | solution.py:36
  609.3 2.5 reshape_reshape_reshape.7
  611.8 2.4 gather_fusion.1
  614.2 2.4 reshape.145
  616.5 3.2 multiply_reduce_fusion
  (229 shorter events, 108.9 us)
Async XLA Ops:
  7.2 240.0 %copy-start = (bf16[1,256,2048]{2,1,0:T(8,128)(2,1)S(1)}, bf16[1,256,2048]{2,1,0:T(8,128)(2,1)}, u32[]{:S(2)}) copy-start(bf16[1,256,2048]{2,1,0:T(8,128)(2,1)} %param.34) | copy-start | bytes 3145732
  20.6 32.0 %copy-start.5 = (bf16[128,2048]{1,0:T(8,128)(2,1)S(1)}, bf16[128,2048]{1,0:T(8,128)(2,1)}, u32[]{:S(2)}) copy-start(bf16[128,2048]{1,0:T(8,128)(2,1)} %param.28) | copy-start | bytes 1572868
  20.6 32.0 %copy-start.11 = (f32[2048]{0:T(1024)S(1)}, f32[2048]{0:T(1024)}, u32[]{:S(2)}) copy-start(f32[2048]{0:T(1024)} %param.29) | copy-start | bytes 24580
  28.5 98.3 %all-to-all-start.2 = ((bf16[16,2,1,1,12,2048]{5,1,4,3,2,0:T(2,128)(2,1)}), bf16[16,2,1,1,12,2048]{5,1,4,3,2,0:T(2,128)(2,1)}, u32[]{:S(2)}, u32[]{:S(2)}) async-start(bf16[16,2,1,1,12,2048]{5,1,4,3,2,0:T(2,128)(2,1)} %copy.87), calls=%async_computation.2 | async-start | bytes 3145728 | tf_op jit(solution)/shard_map/all_to_all | solution.py:36
  52.5 166.1 %all-gather.5.cloned.1.call-start = ((), (), s32[]{:S(2)}) async-start(), calls=%async_computation.7 | async-start | bytes 10485760 | tf_op jit(solution)/shard_map/all_gather | solution.py:174
  129.0 4.7 copy-start.6
  129.0 4.7 copy-start.7
  129.1 4.7 copy-start.8
  130.4 4.6 copy-start.9
  130.4 4.7 copy-start.10
  133.7 173.7 %all-gather.3.cloned.1.call-start = ((), (), s32[]{:S(2)}) async-start(), calls=%async_computation.6 | async-start | bytes 12976128 | tf_op jit(solution)/shard_map/all_gather | solution.py:17
  134.6 367.3 %reduce-scatter.2.cloned.1.call-start = ((), (), s32[]{:S(2)}) async-start(), calls=%async_computation.8 | async-start | bytes 10485760 | tf_op jit(solution)/shard_map/reduce_scatter | solution.py:201
  225.1 10.4 %copy-start.15 = (bf16[1,2048,256]{2,1,0:T(8,128)(2,1)S(1)}, bf16[1,2048,256]{2,1,0:T(8,128)(2,1)}, u32[]{:S(2)}) copy-start(bf16[1,2048,256]{2,1,0:T(8,128)(2,1)} %param.32) | copy-start | bytes 3145732
  264.2 10.5 %copy-start.16 = (bf16[2048,128]{1,0:T(8,128)(2,1)S(1)}, bf16[2048,128]{1,0:T(8,128)(2,1)}, u32[]{:S(2)}) copy-start(bf16[2048,128]{1,0:T(8,128)(2,1)} %param.35) | copy-start | bytes 1572868
  264.2 12.9 %copy-start.17 = (bf16[128,2048]{1,0:T(8,128)(2,1)S(1)}, bf16[128,2048]{1,0:T(8,128)(2,1)}, u32[]{:S(2)}) copy-start(bf16[128,2048]{1,0:T(8,128)(2,1)} %param.37) | copy-start | bytes 1572868
  264.2 12.9 %copy-start.18 = (bf16[2048,128]{1,0:T(8,128)(2,1)S(1)}, bf16[2048,128]{1,0:T(8,128)(2,1)}, u32[]{:S(2)}) copy-start(bf16[2048,128]{1,0:T(8,128)(2,1)} %param.36) | copy-start | bytes 1572868
  382.6 118.1 %copy-start.13 = (f32[2]{0:T(128)S(1)}, f32[2]{0:T(128)}, u32[]{:S(2)}) copy-start(f32[2]{0:T(128)} %param.25) | copy-start | bytes 28
  382.6 118.2 %copy-start.14 = (f32[128]{0:T(128)S(1)}, f32[128]{0:T(128)}, u32[]{:S(2)}) copy-start(f32[128]{0:T(128)} %param.26) | copy-start | bytes 1540
  384.7 3.0 copy-start.2
  387.7 2.1 copy-start.4
  392.8 3.8 copy-start.3
  399.5 2.9 copy-start.2
  402.4 2.1 copy-start.4
  407.6 3.8 copy-start.3
  414.2 2.9 copy-start.2
  417.2 2.1 copy-start.4
  422.3 3.8 copy-start.3
  428.9 2.9 copy-start.2
  431.9 2.1 copy-start.4
  437.0 3.8 copy-start.3
  443.7 2.9 copy-start.2
  446.6 2.1 copy-start.4
  451.8 3.8 copy-start.3
  458.4 2.9 copy-start.2
  461.3 2.1 copy-start.4
  466.5 3.8 copy-start.3
  473.1 2.9 copy-start.2
  476.1 2.1 copy-start.4
  481.2 3.8 copy-start.3
  487.8 2.9 copy-start.2
  490.8 2.1 copy-start.4
  495.9 3.8 copy-start.3
  508.0 26.3 %copy-start.12 = (f32[128,2]{0,1:T(2,128)S(1)}, f32[128,2]{0,1:T(2,128)}, u32[]{:S(2)}) copy-start(f32[128,2]{0,1:T(2,128)} %param.31) | copy-start | bytes 3076
  513.0 10.6 %all-to-all-start = ((bf16[4,96,256]{2,1,0:T(8,128)(2,1)}), bf16[4,96,256]{2,1,0:T(8,128)(2,1)S(1)}, u32[]{:S(2)}, u32[]{:S(2)}) async-start(bf16[4,96,256]{2,1,0:T(8,128)(2,1)} %all_to_all.26), calls=%async_computation | async-start | bytes 393216 | tf_op jit(solution)/shard_map/all_to_all | solution.py:142
  523.6 83.7 %all-to-all-start.4 = ((bf16[16,2,1,12,2048]{4,1,3,2,0:T(2,128)(2,1)}), bf16[16,2,1,12,2048]{4,1,3,2,0:T(2,128)(2,1)S(1)}, u32[]{:S(2)}, u32[]{:S(2)}) async-start(bf16[16,2,1,12,2048]{4,1,3,2,0:T(2,128)(2,1)} %copy.96), calls=%async_computation.5 | async-start | bytes 3145728 | tf_op jit(solution)/shard_map/all_to_all | solution.py:36
  611.8 9.9 %copy-start.1 = (bf16[1,256,2048]{2,1,0:T(8,128)(2,1)S(1)}, bf16[1,256,2048]{2,1,0:T(8,128)(2,1)}, u32[]{:S(2)}) copy-start(bf16[1,256,2048]{2,1,0:T(8,128)(2,1)} %param.34) | copy-start | bytes 3145732
Sparse Core Ops, SparseCore 0:
  133.8 84.7 all-gather.4
  221.0 86.2 all-gather.2
  310.0 83.3 reduce-scatter.1
where the time goes:
time: 638 us; the launch traced here: 629 us
  waiting for transfers between devices  231 us (36%)
  local copies, waits for them, and re-layouts  189 us (30%)
  matrix products  107 us (17%)
  starting transfers between devices  39.4 us (6%)
  other arithmetic  35.5 us (6%)
  between operations  14.7 us (2%)
  blocking collectives  10.2 us (2%)
    all_to_all x2, waiting for transfers between devices, exchange_in_order(): lax.all_to_all(tiles, axes[k], split_axis=k, concat_axis=k, tiled=True)  142 us
    all_gather x1, waiting for transfers between devices, shards(): gathered = lax.all_gather(local_rows, 'tp', axis=0, tiled=True)  83.4 us
    dot_general x16, matrix products, softmax_update(): jnp.einsum('qhk,khe->qhe', weights.astype(jnp.bfloat16), value_block, pre...  35.7 us
    all_to_all x2, starting transfers between devices, exchange_in_order(): lax.all_to_all(tiles, axes[k], split_axis=k, concat_axis=k, tiled=True)  34.7 us
    unnamed x38, local copies, waits for them, and re-layouts  32.3 us
    while x64, local copies, waits for them, and re-layouts  19.1 us
    dynamic_slice x16, local copies, waits for them, and re-layouts, shards(): carried, unused = lax.scan(fold_step, carried, stacked)  17.6 us
    dot_general x1, matrix products, shards(): jnp.einsum('osecf,efd->osecd', hidden, expert_down, preferred_element_typ...  17 us
  transfers between devices with their start and end apart: 6, of which 5 were waited for; matrix products, arithmetic and copies ran while one was open for 43% of the time, Pallas kernels for 0%

commit v1 on v0

--- a/solution.py
+++ b/solution.py
@@ -3,6 +3,7 @@
 from jax import lax
 from jax.sharding import Mesh
 from jax.sharding import PartitionSpec as P
+from jax.lax import all_to_all, axis_size
 
 EP = ("ep_0", "ep_1")
 GRP_EP = ("grp", "ep_0", "ep_1")
@@ -171,7 +172,10 @@
     local_rows = jnp.concatenate(
         [arrived.reshape(1, routed_rows, model_width), normed[None]], axis=1
     )
-    gathered = lax.all_gather(local_rows, "tp", axis=0, tiled=True)
+    series_review = lambda state, net_axis: jnp.concatenate(
+        all_to_all(jnp.stack([state] * axis_size(net_axis), axis=0), net_axis, 0, 0), axis=0
+    )
+    gathered = series_review(local_rows, "tp")
     owners = owner_span * lax.axis_size("tp") // owner_span
     routed_in = gathered[:, :routed_rows].reshape(
         owners, ep_count, local_experts, capacity, model_width

time: 638 us -> 671 us (1.052)
  waiting for transfers between devices: 231 us -> 254 us
    all_to_all x0 -> x1, waiting for transfers between devices: none -> 92.5 us  [shards(): all_to_all(jnp.stack([state] * axis_size(net_axis), axis=0), net_axis, 0, 0)]
    all_gather x1 -> x0, waiting for transfers between devices: 83.4 us -> none  [shards(): gathered = lax.all_gather(local_rows, 'tp', axis=0, tiled=True)]
    all_to_all x2, waiting for transfers between devices: 142 us -> 157 us  [exchange_in_order(): lax.all_to_all(tiles, axes[k], split_axis=k, concat_axis=k, tiled=True)]
    unnamed x38 -> x32, local copies, waits for them, and re-layouts: 32.3 us -> 32.2 us
  transfers between devices with their start and end apart: 6 -> 6, of which waited for: 5 -> 4; matrix products, arithmetic and copies ran while one was open for 43% -> 44% of each run, Pallas kernels for 0% -> 0%
where the time goes in v1:
time: 671 us; the launch traced here: 661 us
  waiting for transfers between devices  254 us (38%)
  local copies, waits for them, and re-layouts  193 us (29%)
  matrix products  107 us (16%)
  starting transfers between devices  44.3 us (7%)
  other arithmetic  35.1 us (5%)
  between operations  16.4 us (2%)
  blocking collectives  10.2 us (2%)
    all_to_all x2, waiting for transfers between devices, exchange_in_order(): lax.all_to_all(tiles, axes[k], split_axis=k, concat_axis=k, tiled=True)  157 us
    all_to_all x1, waiting for transfers between devices, shards(): all_to_all(jnp.stack([state] * axis_size(net_axis), axis=0), net_axis, 0, 0)  92.5 us
    dot_general x16, matrix products, softmax_update(): jnp.einsum('qhk,khe->qhe', weights.astype(jnp.bfloat16), value_block, pre...  35.7 us
    all_to_all x2, starting transfers between devices, exchange_in_order(): lax.all_to_all(tiles, axes[k], split_axis=k, concat_axis=k, tiled=True)  34.6 us
    unnamed x32, local copies, waits for them, and re-layouts  32.2 us
    while x64, local copies, waits for them, and re-layouts  19 us
    dynamic_slice x16, local copies, waits for them, and re-layouts, shards(): carried, unused = lax.scan(fold_step, carried, stacked)  17.6 us
    dot_general x8, matrix products, fold_step(): jnp.einsum('qhd,khd->qhk', query_two, key_b, preferred_element_type=jnp.f...  17 us
  transfers between devices with their start and end apart: 6, of which 4 were waited for; matrix products, arithmetic and copies ran while one was open for 44% of the time, Pallas kernels for 0%

profile of v1, /device:TPU:40, one launch (start us, length us, event | category | flops | bytes accessed | tf_op | source)
XLA Modules:
  0.0 660.7 jit_solution(41283349972062078)
XLA Ops:
  17.0 3.1 gather_fusion
  20.1 2.4 reshape_transpose_reshape_reshape.3
  23.4 5.1 all_to_all.44
  28.5 2.8 copy.87
  31.3 24.3 %all-to-all-start.2 = ((bf16[16,2,1,1,12,2048]{5,1,4,3,2,0:T(2,128)(2,1)}), bf16[16,2,1,1,12,2048]{5,1,4,3,2,0:T(2,128)(2,1)}, u32[]{:S(2)}, u32[]{:S(2)}) async-start(bf16[16,2,1,1,12,2048]{5,1,4,3,2,0:T(2,128)(2,1)} %copy.87), calls=%async_computation.2 | async-start | bytes 3145728 | tf_op jit(solution)/shard_map/all_to_all | solution.py:37
  56.6 88.0 %all-to-all-done.2 = bf16[16,2,1,1,12,2048]{5,1,4,3,2,0:T(2,128)(2,1)} async-done(((bf16[16,2,1,1,12,2048]{5,1,4,3,2,0:T(2,128)(2,1)}), bf16[16,2,1,1,12,2048]{5,1,4,3,2,0:T(2,128)(2,1)}, u32[]{:S(2)}, u32[]{:S(2)}) %all-to-all-start.2) | async-done | bytes 1572896 | tf_op jit(solution)/shard_map/all_to_all | solution.py:37
  149.9 4.3 stack.2
  154.2 5.9 all-to-all-start.3
  160.7 92.5 %all-to-all-done.3 = bf16[4,1,512,2048]{3,2,1,0:T(8,128)(2,1)} async-done(((bf16[4,1,512,2048]{3,2,1,0:T(8,128)(2,1)}), bf16[4,1,512,2048]{3,2,1,0:T(8,128)(2,1)}, u32[]{:S(2)}, u32[]{:S(2)}) %all-to-all-start.3) | async-done | bytes 8388640 | tf_op jit(solution)/shard_map/all_to_all | solution.py:176
  253.3 6.5 slice.34
  259.8 10.4 %copy.89 = bf16[4,384,2048]{2,0,1:T(4,128)(2,1)} copy(bf16[4,384,2048]{2,1,0:T(8,128)(2,1)} %slice.34) | data formatting | bytes 12582912 | tf_op jit(solution)/shard_map/slice | solution.py:180
  270.1 11.4 %fusion.44 = f32[4,32,12,256]{3,1,2,0:T(8,128)} fusion(bf16[4,32,12,2048]{3,0,2,1:T(4,128)(2,1)} %bitcast.194, bf16[1,2048,256]{2,1,0:T(8,128)(2,1)S(1)} %copy-done.12), kind=kOutput, calls=%fused_computation.52 | convolution fusion | flops 1610612736 | bytes 8912896 | tf_op jit(solution)/shard_map/osecd,edf->osecf/dot_general | solution.py:183
  281.5 16.8 %convert_bitcast_fusion = bf16[4,32,1,12,2048]{4,1,3,0,2:T(8,128)(2,1)} fusion(bf16[1,256,2048]{2,1,0:T(8,128)(2,1)S(1)} %copy-done, bf16[4,32,12,2048]{3,0,2,1:T(4,128)(2,1)} %bitcast.195, f32[4,32,12,256]{3,1,2,0:T(8,128)} %fusion.44, bf16[1,2048,256]{2,1,0:T(8,128)(2,1)} %param.33), kind=kOutput, calls=%fused_computation.49 | convolution fusion | flops 3226730496 | bytes 16252928 | tf_op jit(solution)/shard_map/osecf,efd->osecd/dot_general | solution.py:190
  298.3 10.4 %copy.92 = bf16[4,32,1,12,2048]{4,0,3,1,2:T(4,128)(2,1)} copy(bf16[4,32,1,12,2048]{4,1,3,0,2:T(8,128)(2,1)} %convert_bitcast_fusion) | data formatting | bytes 12582912 | tf_op jit(solution)/shard_map/osecf,efd->osecd/transpose | solution.py:190
  308.8 2.3 fusion.48
  311.1 5.2 convolution_convert_fusion
  316.3 3.2 copy.93
  319.5 8.4 %pad_maximum_fusion = bf16[4,512,2048]{2,0,1:T(4,128)(2,1)} fusion(bf16[4,128,2048]{2,0,1:T(4,128)(2,1)S(1)} %copy.93, bf16[4,384,2048]{2,0,1:T(4,128)(2,1)} %bitcast.193), kind=kLoop, calls=%fused_computation.48 | loop fusion | flops 4194304 | bytes 16777216 | tf_op jit(solution)/shard_map/concatenate | solution.py:206
  327.9 11.3 %copy.94 = bf16[4,512,2048]{2,1,0:T(8,128)(2,1)} copy(bf16[4,512,2048]{2,0,1:T(4,128)(2,1)} %pad_maximum_fusion) | data formatting | bytes 16777216 | tf_op jit(solution)/shard_map/concatenate | solution.py:206
  339.3 4.8 fusion.94
  344.1 11.6 %reshape.184 = bf16[8,1536,2,64]{3,2,1,0:T(2,128)(2,1)} reshape(bf16[12288,128]{1,0:T(8,128)(2,1)} %get-tuple-element.183) | data formatting | bytes 6291456 | tf_op jit(solution)/shard_map/reshape | solution.py:108
  355.8 15.5 %copy.77 = bf16[8,1536,2,64]{1,3,2,0:T(8,128)(2,1)} copy(bf16[8,1536,2,64]{3,2,1,0:T(2,128)(2,1)} %reshape.184) | data formatting | bytes 6291456
  371.2 11.6 %reshape.186 = bf16[8,1536,2,64]{3,2,1,0:T(2,128)(2,1)} reshape(bf16[12288,128]{1,0:T(8,128)(2,1)} %get-tuple-element.182) | data formatting | bytes 6291456 | tf_op jit(solution)/shard_map/reshape | solution.py:109
  382.8 15.5 %copy.79 = bf16[8,1536,2,64]{1,3,2,0:T(8,128)(2,1)} copy(bf16[8,1536,2,64]{3,2,1,0:T(2,128)(2,1)} %reshape.186) | data formatting | bytes 6291456
  398.4 6.4 split.13
  404.8 9.8 %reshape.185 = bf16[8,1536,2,128]{3,2,1,0:T(2,128)(2,1)} reshape(bf16[12288,256]{1,0:T(8,128)(2,1)} %split.13) | data formatting | bytes 12582912 | tf_op jit(solution)/shard_map/reshape | solution.py:110
  414.6 118.0 %while.21 = (s32[]{:T(128)}, f32[384,2]{0,1:T(2,128)S(1)}, f32[384,2]{0,1:T(2,128)S(1)}, f32[384,2,128]{0,2,1:T(8,128)S(1)}, f32[384,2]{0,1:T(2,128)S(1)}, /*ind...) while((s32[]{:T(128)}, f32[384,2]{0,1:T(2,128)S(1)}, ...), condition=%wide.region_5.6_spmd.clone, body=%wide.region_0.5_spmd.clone.sunk | while | flops 925441536 | bytes 92308720 | solution.py:132
  424.8 3.5 fusion.125
  439.5 3.5 fusion.125
  454.2 3.5 fusion.125
  468.9 3.5 fusion.125
  483.6 3.5 fusion.125
  498.4 3.5 fusion.125
  513.1 3.5 fusion.125
  527.8 3.5 fusion.125
  533.8 2.7 slice.36
  536.6 2.4 reshape_reshape_reshape.6
  539.8 5.0 all_to_all.45
  544.8 3.5 all-to-all-start
  548.3 2.8 copy.96
  551.1 3.7 all-to-all-done
  554.8 10.3 %all-to-all-start.5 = ((bf16[16,2,1,12,2048]{4,1,3,2,0:T(2,128)(2,1)}), bf16[16,2,1,12,2048]{4,1,3,2,0:T(2,128)(2,1)S(1)}, u32[]{:S(2)}, u32[]{:S(2)}) async-start(bf16[16,2,1,12,2048]{4,1,3,2,0:T(2,128)(2,1)} %copy.96), calls=%async_computation.6 | async-start | bytes 3145728 | tf_op jit(solution)/shard_map/all_to_all | solution.py:37
  565.3 3.7 convolution_convert_fusion.1
  569.0 69.3 %all-to-all-done.5 = bf16[16,2,1,12,2048]{4,1,3,2,0:T(2,128)(2,1)S(1)} async-done(((bf16[16,2,1,12,2048]{4,1,3,2,0:T(2,128)(2,1)}), bf16[16,2,1,12,2048]{4,1,3,2,0:T(2,128)(2,1)S(1)}, u32[]{:S(2)}, u32[]{:S(2)}) %all-to-all-start.5) | async-done | bytes 1572896 | tf_op jit(solution)/shard_map/all_to_all | solution.py:37
  640.4 2.5 reshape_reshape_reshape.7
  642.9 2.3 gather_fusion.1
  645.3 2.4 reshape.152
  647.6 3.2 multiply_reduce_fusion
  (223 shorter events, 112.0 us)
Async XLA Ops:
  8.0 273.5 %copy-start = (bf16[1,256,2048]{2,1,0:T(8,128)(2,1)S(1)}, bf16[1,256,2048]{2,1,0:T(8,128)(2,1)}, u32[]{:S(2)}) copy-start(bf16[1,256,2048]{2,1,0:T(8,128)(2,1)} %param.34) | copy-start | bytes 3145732
  8.1 331.2 %all-gather.2.cloned.1.call-start = ((), (), s32[]{:S(2)}) async-start(), calls=%async_computation.7 | async-start | bytes 12976128 | tf_op jit(solution)/shard_map/all_gather | solution.py:18
  23.4 32.2 %copy-start.5 = (bf16[128,2048]{1,0:T(8,128)(2,1)S(1)}, bf16[128,2048]{1,0:T(8,128)(2,1)}, u32[]{:S(2)}) copy-start(bf16[128,2048]{1,0:T(8,128)(2,1)} %param.28) | copy-start | bytes 1572868
  23.4 32.2 %copy-start.8 = (f32[2048]{0:T(1024)S(1)}, f32[2048]{0:T(1024)}, u32[]{:S(2)}) copy-start(f32[2048]{0:T(1024)} %param.29) | copy-start | bytes 24580
  31.3 113.2 %all-to-all-start.2 = ((bf16[16,2,1,1,12,2048]{5,1,4,3,2,0:T(2,128)(2,1)}), bf16[16,2,1,1,12,2048]{5,1,4,3,2,0:T(2,128)(2,1)}, u32[]{:S(2)}, u32[]{:S(2)}) async-start(bf16[16,2,1,1,12,2048]{5,1,4,3,2,0:T(2,128)(2,1)} %copy.87), calls=%async_computation.2 | async-start | bytes 3145728 | tf_op jit(solution)/shard_map/all_to_all | solution.py:37
  154.2 6.2 copy-start.6
  154.2 6.4 copy-start.7
  154.2 99.1 %all-to-all-start.3 = ((bf16[4,1,512,2048]{3,2,1,0:T(8,128)(2,1)}), bf16[4,1,512,2048]{3,2,1,0:T(8,128)(2,1)}, u32[]{:S(2)}, u32[]{:S(2)}) async-start(bf16[4,1,512,2048]{3,2,1,0:T(8,128)(2,1)} %stack.2), calls=%async_computation.3 | async-start | bytes 16777216 | tf_op jit(solution)/shard_map/all_to_all | solution.py:176
  160.1 373.7 %reduce-scatter.2.cloned.1.call-start = ((), (), s32[]{:S(2)}) async-start(), calls=%async_computation.8 | async-start | bytes 10485760 | tf_op jit(solution)/shard_map/reduce_scatter | solution.py:205
  259.8 10.4 %copy-start.12 = (bf16[1,2048,256]{2,1,0:T(8,128)(2,1)S(1)}, bf16[1,2048,256]{2,1,0:T(8,128)(2,1)}, u32[]{:S(2)}) copy-start(bf16[1,2048,256]{2,1,0:T(8,128)(2,1)} %param.32) | copy-start | bytes 3145732
  298.3 10.4 %copy-start.13 = (bf16[2048,128]{1,0:T(8,128)(2,1)S(1)}, bf16[2048,128]{1,0:T(8,128)(2,1)}, u32[]{:S(2)}) copy-start(bf16[2048,128]{1,0:T(8,128)(2,1)} %param.35) | copy-start | bytes 1572868
  298.3 12.7 %copy-start.14 = (bf16[128,2048]{1,0:T(8,128)(2,1)S(1)}, bf16[128,2048]{1,0:T(8,128)(2,1)}, u32[]{:S(2)}) copy-start(bf16[128,2048]{1,0:T(8,128)(2,1)} %param.37) | copy-start | bytes 1572868
  298.3 12.7 %copy-start.15 = (bf16[2048,128]{1,0:T(8,128)(2,1)S(1)}, bf16[2048,128]{1,0:T(8,128)(2,1)}, u32[]{:S(2)}) copy-start(bf16[2048,128]{1,0:T(8,128)(2,1)} %param.36) | copy-start | bytes 1572868
  414.6 118.0 %copy-start.10 = (f32[2]{0:T(128)S(1)}, f32[2]{0:T(128)}, u32[]{:S(2)}) copy-start(f32[2]{0:T(128)} %param.25) | copy-start | bytes 28
  414.6 118.2 %copy-start.11 = (f32[128]{0:T(128)S(1)}, f32[128]{0:T(128)}, u32[]{:S(2)}) copy-start(f32[128]{0:T(128)} %param.26) | copy-start | bytes 1540
  416.6 2.9 copy-start.2
  419.6 2.1 copy-start.4
  424.7 3.8 copy-start.3
  431.4 2.9 copy-start.2
  434.3 2.1 copy-start.4
  439.5 3.8 copy-start.3
  446.1 2.9 copy-start.2
  449.1 2.1 copy-start.4
  454.2 3.8 copy-start.3
  460.8 2.9 copy-start.2
  463.8 2.1 copy-start.4
  468.9 3.8 copy-start.3
  475.5 2.9 copy-start.2
  478.5 2.1 copy-start.4
  483.6 3.8 copy-start.3
  490.3 2.9 copy-start.2
  493.2 2.1 copy-start.4
  498.3 3.8 copy-start.3
  505.0 2.9 copy-start.2
  507.9 2.1 copy-start.4
  513.1 3.8 copy-start.3
  519.7 2.9 copy-start.2
  522.6 2.1 copy-start.4
  527.8 3.8 copy-start.3
  539.8 25.3 %copy-start.9 = (f32[128,2]{0,1:T(2,128)S(1)}, f32[128,2]{0,1:T(2,128)}, u32[]{:S(2)}) copy-start(f32[128,2]{0,1:T(2,128)} %param.31) | copy-start | bytes 3076
  544.8 9.9 %all-to-all-start = ((bf16[4,96,256]{2,1,0:T(8,128)(2,1)}), bf16[4,96,256]{2,1,0:T(8,128)(2,1)S(1)}, u32[]{:S(2)}, u32[]{:S(2)}) async-start(bf16[4,96,256]{2,1,0:T(8,128)(2,1)} %all_to_all.29), calls=%async_computation | async-start | bytes 393216 | tf_op jit(solution)/shard_map/all_to_all | solution.py:143
  554.8 83.5 %all-to-all-start.5 = ((bf16[16,2,1,12,2048]{4,1,3,2,0:T(2,128)(2,1)}), bf16[16,2,1,12,2048]{4,1,3,2,0:T(2,128)(2,1)S(1)}, u32[]{:S(2)}, u32[]{:S(2)}) async-start(bf16[16,2,1,12,2048]{4,1,3,2,0:T(2,128)(2,1)} %copy.96), calls=%async_computation.6 | async-start | bytes 3145728 | tf_op jit(solution)/shard_map/all_to_all | solution.py:37
  642.9 9.9 %copy-start.1 = (bf16[1,256,2048]{2,1,0:T(8,128)(2,1)S(1)}, bf16[1,256,2048]{2,1,0:T(8,128)(2,1)}, u32[]{:S(2)}) copy-start(bf16[1,256,2048]{2,1,0:T(8,128)(2,1)} %param.34) | copy-start | bytes 3145732
Sparse Core Ops, SparseCore 0:
  11.3 165.8 all-gather.1
Sparse Core Ops, SparseCore 1:
  339.4 83.5 reduce-scatter.1
